TPU v7x, 32 devices: a whole 2x2x4 slice. The times are simulated.
32 devices in a mesh: grp: 2 (over x), ep: 8 (over z, y), tp: 2 (over core).
Axes of the slice: x: 2, y: 2, z: 4, core: 2. Of those that a mesh axis runs over, the one named last changes fastest.
Arguments:
- tokens: bfloat16 [3072, 2048], P(('grp', 'ep'), 'tp'), parts along dimension 0, may hold values from -10 to 10
- gain_in: float32 [2048], replicated, may hold values from 0.1 to 1.9
- gain_out: float32 [2048], replicated, may hold values from 0.1 to 1.9
- expert_ids: int32 [3072, 2], P(('grp', 'ep')), parts along dimension 0, may hold values from 0 to 3, all different within a row; in each aligned block of 192 rows (0 to 191, 192 to 383, ...) at most 144 rows name the same one
- route_weight: float32 [3072, 2], P(('grp', 'ep')), parts along dimension 0, may hold values from 0.1 to 1
- gate_weight: bfloat16 [8, 2048, 1792], P('ep', None, 'tp'), may hold values from -0.125 to 0.125
- up_weight: bfloat16 [8, 2048, 1792], P('ep', None, 'tp'), may hold values from -0.125 to 0.125
- down_weight: bfloat16 [8, 1792, 2048], P('ep', 'tp'), may hold values from -1 to 1
Outputs:
- layer_out: bfloat16 [3072, 2048], P(('grp', 'ep'), 'tp'), parts along dimension 0
There are 2 independent parts, one for each index of `grp`. A program takes and returns all parts, laid end to end along the dimension named above; an argument that names none is the same for every part. Nothing has to cross between parts.
Inputs may be any that keep to these rules, and one draw needn't show every extreme that they name: `expert_ids`: each row names 2 different experts. Among the tokens of one index of ep no expert is named more than 144 times, a bound that some block reaches.
All inputs are finite; a program needn't handle non-finite values.
Results may differ from a plain program's by a relative error of at most 0.0077.
Values may be sent and summed in bfloat16 or wider, within the bound.
A program may use at most 64 MiB of HBM per device.

v0:
```python
import functools

import jax
import jax.numpy as jnp
from jax import lax
from jax.experimental import pallas as pl
from jax.experimental.pallas import tpu as pltpu
from jax.sharding import PartitionSpec as P

norm_eps = 1e-06


def plain(
    tokens, gain_in, gain_out, expert_ids, route_weight, gate_weight, up_weight, down_weight
):
    tok_rows, half_width = tokens.shape
    full_width = 2 * half_width
    expert_count = lax.axis_size("ep") // 2
    picks = expert_ids.shape[1]
    capacity = tok_rows * picks * 3 // (2 * expert_count)
    own_cols = lax.axis_index("tp") * half_width
    own_float = tokens.astype(jnp.float32)
    squares = lax.psum(jnp.sum(own_float * own_float, axis=1), "tp")
    factor = lax.rsqrt(squares / full_width + norm_eps)[:, None]
    own_gain = lax.dynamic_slice_in_dim(gain_in, own_cols, half_width)
    normed = (own_float * factor * own_gain).astype(jnp.bfloat16)
    sent_width = normed.shape[1]
    flat_ids = expert_ids.reshape(-1)
    onehot = (flat_ids[:, None] == jnp.arange(expert_count, dtype=jnp.int32)[None, :]).astype(
        jnp.int32
    )
    before = jnp.cumsum(onehot, axis=0) - onehot
    targets = flat_ids * capacity + jnp.sum(before * onehot, axis=1)
    per_token = targets.reshape(tok_rows, picks)
    slot_rows = jnp.arange(expert_count * capacity, dtype=jnp.int32)[:, None]
    placing = jnp.zeros((expert_count * capacity, tok_rows), jnp.bfloat16)
    for which in range(picks):
        placing = placing + (slot_rows == per_token[None, :, which]).astype(jnp.bfloat16)
    packed = jnp.dot(placing, normed, preferred_element_type=jnp.float32).astype(jnp.bfloat16)
    stacked = packed.reshape(expert_count, 1, capacity, sent_width)
    outgoing = jnp.broadcast_to(stacked, (expert_count, 2, capacity, sent_width)).reshape(
        2 * expert_count, capacity, sent_width
    )
    arrived = lax.all_to_all(outgoing, "ep", split_axis=0, concat_axis=0, tiled=True)
    arrived = lax.all_gather(arrived, "tp", axis=2, tiled=True)
    sources = arrived.shape[0]
    gathered = arrived.reshape(sources * capacity, full_width)
    gate_pre = jnp.dot(gathered, gate_weight[0], preferred_element_type=jnp.float32)
    up_pre = jnp.dot(gathered, up_weight[0], preferred_element_type=jnp.float32)
    hidden = (jax.nn.silu(gate_pre) * up_pre).astype(jnp.bfloat16)
    partial_value = jnp.dot(hidden, down_weight[0], preferred_element_type=jnp.float32).astype(
        jnp.bfloat16
    )
    partial_value = partial_value.reshape(sources, capacity, full_width)
    half_sum = lax.psum_scatter(partial_value, "tp", scatter_dimension=2, tiled=True).astype(
        jnp.float32
    )
    returned = lax.all_to_all(
        half_sum.astype(jnp.bfloat16), "ep", split_axis=0, concat_axis=0, tiled=True
    )
    merged = jnp.sum(
        returned.reshape(expert_count, 2, capacity, half_width).astype(jnp.float32), axis=1
    )
    merged = merged.reshape(expert_count * capacity, half_width)
    picked = jnp.take(merged, targets, axis=0).reshape(tok_rows, picks, half_width)
    routed = jnp.sum(picked * route_weight[:, :, None], axis=1)
    squares_out = lax.psum(jnp.sum(routed * routed, axis=1), "tp")
    factor_out = lax.rsqrt(squares_out / full_width + norm_eps)[:, None]
    own_gain_out = lax.dynamic_slice_in_dim(gain_out, own_cols, half_width)
    return (routed * factor_out * own_gain_out).astype(jnp.bfloat16)


MESH = pl.DeviceIdType.MESH


def fused(
    experts,
    cap,
    tok_ref,
    gain_in_ref,
    gain_out_ref,
    ids_ref,
    route_ref,
    gate_hbm,
    up_hbm,
    down_hbm,
    out_ref,
    arrived,
    notes,
    rows,
    parts,
    peer_parts,
    crossing,
    crossed,
    leaving,
    home,
    gate_up,
    down,
    squared,
    peer_squared,
    sums,
    peer_sums,
    total,
    w_sem,
    sq_send,
    sq_recv,
    own_send,
    own_note_send,
    note_send,
    note_recv,
    line_send,
    line_recv,
    core_send,
    core_recv,
    pair_send,
    pair_recv,
    relay_send,
    relay_recv,
    part_send,
    part_recv,
    cross_send,
    cross_recv,
    home_send,
    home_recv,
):
    tok_rows, width = tok_ref.shape
    hidden_width = down.shape[0]
    place = lax.axis_index("ep")
    core = lax.axis_index("tp")
    half = place % 2
    mine = place // 2
    partner = place + 1 - 2 * half
    other = 1 - core
    own_cols = pl.ds(pl.multiple_of(core * width, 128), width)
    other_cols = pl.ds(pl.multiple_of(other * width, 128), width)

    size = ((cap // 16 + 1) // 2 * 16, cap // 16 // 2 * 16)
    begin = (0, size[0])

    def unit(h):
        return pl.ds(begin[h], size[h])

    def side_unit(h, which):
        return pl.ds(2 * begin[h] + which * size[h], size[h])

    def both(h):
        return pl.ds(2 * begin[h], 2 * size[h])

    piece = width // 2

    def cut(p):
        return pl.ds(p * piece, piece)

    def of_core(which, p):
        return pl.ds(pl.multiple_of(which * width + p * piece, 128), piece)

    def turn(where):
        return 1 - 2 * ((2 * where) // experts)

    at_end = (mine == 0) | (mine == experts - 1)
    inner = jnp.logical_not(at_end)

    def at_step(step):
        far = jnp.where(step == 2, experts - 1, jnp.where(step > 2, step - 1, step))
        count = jnp.where(inner, far, step)
        return (mine + turn(mine) * count + experts) % experts

    def on_line(there):
        return {"ep": 2 * there + half}

    loads = [
        pltpu.make_async_copy(gate_hbm.at[0], gate_up.at[:, pl.ds(0, hidden_width)], w_sem.at[0]),
        pltpu.make_async_copy(
            up_hbm.at[0], gate_up.at[:, pl.ds(hidden_width, hidden_width)], w_sem.at[1]
        ),
        pltpu.make_async_copy(down_hbm.at[0], down, w_sem.at[2]),
    ]
    barrier = pltpu.get_barrier_semaphore()
    sides = (-1, 1)

    def inside(where):
        return (where >= 0) & (where < experts)

    def greet(side):
        there = on_line(mine + side)
        pl.semaphore_signal(barrier, inc=1, device_id=there, device_id_type=MESH)

    for side in sides:
        pl.when(inside(mine + side))(functools.partial(greet, side))
    pl.semaphore_signal(barrier, inc=1, device_id={"ep": partner}, device_id_type=MESH)
    pl.semaphore_signal(barrier, inc=1, device_id={"tp": other}, device_id_type=MESH)
    for load in loads:
        load.start()

    def remote(source, target, send, recv, device):
        return pltpu.make_async_remote_copy(
            src_ref=source,
            dst_ref=target,
            send_sem=send,
            recv_sem=recv,
            device_id=device,
            device_id_type=MESH,
        )

    def square_copy():
        return remote(squared, peer_squared, sq_send.at[0], sq_recv.at[0], {"tp": other})

    def sum_copy():
        return remote(sums, peer_sums, sq_send.at[1], sq_recv.at[1], {"tp": other})

    def own_copy(side, p):
        return remote(
            tok_ref.at[:, cut(p)],
            arrived.at[mine, :, cut(p)],
            own_send.at[side + 1 + p],
            line_recv.at[2 * mine + p],
            on_line(mine + side),
        )

    def own_note(side):
        return remote(
            notes.at[mine],
            notes.at[mine],
            own_note_send.at[(side + 1) // 2],
            note_recv.at[mine],
            on_line(mine + side),
        )

    def line_copy(source, p, there):
        view, sem = arrived.at[source, :, cut(p)], 2 * source + p
        return remote(view, view, line_send.at[sem], line_recv.at[sem], on_line(there))

    def note_copy(source, there):
        view = notes.at[source]
        return remote(view, view, note_send.at[source], note_recv.at[source], on_line(there))

    def core_copy(d, p, which):
        view, sem = rows.at[d, 0, :, of_core(which, p)], 2 * d + p
        return remote(view, view, core_send.at[sem], core_recv.at[sem], {"tp": other})

    def pair_copy(d, p):
        return remote(
            rows.at[d, 0, :, of_core(core, p)],
            rows.at[d, 1, :, of_core(core, p)],
            pair_send.at[2 * d + p],
            pair_recv.at[2 * d + p],
            {"ep": partner},
        )

    def relay_copy(d, p, which):
        view, sem = rows.at[d, 1, :, of_core(which, p)], 2 * d + p
        return remote(view, view, relay_send.at[sem], relay_recv.at[sem], {"tp": other})

    def part_copy(d, h):
        return remote(
            parts.at[d, both(h), other_cols],
            peer_parts.at[d, both(h)],
            part_send.at[2 * d + h],
            part_recv.at[2 * d + h],
            {"tp": other},
        )

    def cross_copy(d, h):
        return remote(
            crossing.at[d, unit(h)],
            crossed.at[d, unit(h)],
            cross_send.at[2 * d + h],
            cross_recv.at[2 * d + h],
            {"ep": partner},
        )

    def home_copy(d, h):
        return remote(
            leaving.at[d, unit(h)],
            home.at[mine, unit(h)],
            home_send.at[2 * d + h],
            home_recv.at[2 * mine + h],
            on_line(d),
        )

    def home_arrival(expert, h):
        view, sem = home.at[expert, unit(h)], 2 * expert + h
        return remote(view, view, home_send.at[sem], home_recv.at[sem], on_line(expert))

    own_float = tok_ref[...].astype(jnp.float32)
    squares = jnp.broadcast_to(
        jnp.sum(own_float * own_float, axis=1, keepdims=True), (tok_rows, 128)
    )
    squared[...] = squares.T[0:8, :]
    lead = max(8, experts)
    names = lax.broadcasted_iota(jnp.int32, (lead, tok_rows), 0)
    first = names == ids_ref[0:1, :]
    second = names == ids_ref[1:2, :]
    either = (first.astype(jnp.float32) + second.astype(jnp.float32)).astype(jnp.bfloat16)
    earlier = (
        lax.broadcasted_iota(jnp.int32, (tok_rows, tok_rows), 0)
        < lax.broadcasted_iota(jnp.int32, (tok_rows, tok_rows), 1)
    ).astype(jnp.float32).astype(jnp.bfloat16)
    before = jnp.dot(either, earlier, preferred_element_type=jnp.float32)
    slot_one = jnp.sum(jnp.where(first, before, 0.0), axis=0, keepdims=True).astype(jnp.int32)
    slot_two = jnp.sum(jnp.where(second, before, 0.0), axis=0, keepdims=True).astype(jnp.int32)
    target_one = (ids_ref[0:1, :] * cap + slot_one).astype(jnp.float32)
    target_two = (ids_ref[1:2, :] * cap + slot_two).astype(jnp.float32)

    def slots(expert, first_row, count):
        names = lax.broadcasted_iota(jnp.int32, (count, tok_rows), 0) + expert * cap + first_row
        return names.astype(jnp.float32)

    with jax.named_scope("barrier"):
        pl.semaphore_wait(
            barrier, 2 + (mine > 0).astype(jnp.int32) + (mine < experts - 1).astype(jnp.int32)
        )
    square_copy().start()

    def own_out(side, p):
        own_copy(side, p).start()

    def own_note_out(side):
        own_note(side).start()

    for side in sides:
        pl.when(inside(mine + side))(functools.partial(own_out, side, 0))
    with jax.named_scope("sum0"):
        square_copy().wait_recv()
    factor = lax.rsqrt((squared[...] + peer_squared[...]) / (2 * width) + norm_eps)
    row = lax.broadcasted_iota(jnp.int32, (8, tok_rows), 0)
    notes[mine] = jnp.where(row == 0, target_one, jnp.where(row == 1, target_two, factor))
    for side in sides:
        pl.when(inside(mine + side))(functools.partial(own_note_out, side))
    for side in sides:
        pl.when(inside(mine + side))(functools.partial(own_out, side, 1))

    def fill(source, p, tokens):
        one, two, scale = (notes[source, i : i + 1, :] for i in range(3))
        names = slots(mine, 0, cap)
        placing = jnp.where((names == one) | (names == two), scale, 0.0)
        high = placing.astype(jnp.bfloat16)
        low = (placing - high.astype(jnp.float32)).astype(jnp.bfloat16)
        values = jnp.dot(high, tokens, preferred_element_type=jnp.float32) + jnp.dot(
            low, tokens, preferred_element_type=jnp.float32
        )
        rows[source, 0, :, of_core(core, p)] = (
            values * gain_in_ref[:, of_core(core, p)]
        ).astype(jnp.bfloat16)
        pair_copy(source, p).start()
        core_copy(source, p, core).start()

    def fill_step(step, p):
        source = at_step(step)
        fill(source, p, arrived[source, :, cut(p)])

    def pass_on(step, side, p):
        source, there = mine + side * step, mine - side
        with jax.named_scope("linewait"):
            line_copy(source, p, mine).wait_recv()
        pl.when(inside(there))(lambda: line_copy(source, p, there).start())
        if p == 0:
            with jax.named_scope("notewait"):
                note_copy(source, mine).wait_recv()
            pl.when(inside(there))(lambda: note_copy(source, there).start())

    def take_line(step, p):
        for side in sides:
            pl.when(inside(mine + side * step))(functools.partial(pass_on, step, side, p))

    def take_pair(d):
        for p in range(2):
            with jax.named_scope("pairwait"):
                pair_copy(d, p).wait_recv()
            relay_copy(d, p, core).start()

    def take_core(d):
        with jax.named_scope("corewait"):
            for p in range(2):
                core_copy(d, p, other).wait_recv()
                relay_copy(d, p, other).wait_recv()

    def compute(d, h):
        block = jnp.concatenate([rows[d, 0, unit(h), :], rows[d, 1, unit(h), :]], axis=0)
        pre = jnp.dot(block, gate_up[...], preferred_element_type=jnp.float32)
        gate_pre = pre[:, :hidden_width]
        hidden = (gate_pre / (1.0 + jnp.exp(-gate_pre)) * pre[:, hidden_width:]).astype(
            jnp.bfloat16
        )
        partial = jnp.dot(hidden, down[...], preferred_element_type=jnp.float32)
        parts[d, both(h), :] = partial.astype(jnp.bfloat16)
        part_copy(d, h).start()

    def cross(d, h):
        with jax.named_scope("partwait"):
            part_copy(d, h).wait_recv()
        crossing[d, unit(h)] = (
            parts[d, side_unit(h, 1), own_cols].astype(jnp.float32)
            + peer_parts[d, side_unit(h, 1)].astype(jnp.float32)
        ).astype(jnp.bfloat16)
        cross_copy(d, h).start()

    def meet(d, h):
        with jax.named_scope("crosswait"):
            cross_copy(d, h).wait_recv()
        return (
            parts[d, side_unit(h, 0), own_cols].astype(jnp.float32)
            + peer_parts[d, side_unit(h, 0)].astype(jnp.float32)
            + crossed[d, unit(h)].astype(jnp.float32)
        ).astype(jnp.bfloat16)

    def send_home(d, h):
        leaving[d, unit(h)] = meet(d, h)
        home_copy(d, h).start()

    last = experts - 1
    for p in range(2):
        fill(mine, p, tok_ref[:, cut(p)])
    take_line(1, 0)
    fill_step(1, 0)
    take_pair(mine)
    take_line(1, 1)
    fill_step(1, 1)

    def fill_both(step):
        for p in range(2):
            fill_step(step, p)

    pl.when(inner)(lambda: fill_both(2))
    with jax.named_scope("wwait"):
        for load in loads:
            load.wait()

    def step_of(d, carry):
        now, past = at_step(d), at_step(d - 1)
        early = (d >= 2) | ((d == 1) & inner)
        early_past = (d >= 3) | ((d == 2) & inner)

        def next_line():
            take_line(d + 1, 1)
            pl.when(at_end)(lambda: fill_step(d + 1, 1))

        pl.when(d >= 1)(lambda: take_pair(now))
        pl.when((d >= 2) & (d < last))(next_line)
        take_core(now)
        compute(now, 0)
        pl.when(early_past)(lambda: send_home(past, 0))
        pl.when(d == 1)(next_line)
        compute(now, 1)
        pl.when(early)(lambda: cross(now, 0))
        pl.when(d + 2 <= last)(lambda: take_line(d + 2, 0))
        pl.when(early_past)(lambda: send_home(past, 1))
        pl.when(early)(lambda: cross(now, 1))
        pl.when((d + 2 <= last) & at_end)(lambda: fill_step(d + 2, 0))
        pl.when((d >= 1) & (d + 2 <= last) & inner)(lambda: fill_both(d + 2))
        return carry

    lax.fori_loop(0, experts, step_of, 0)

    def weights_of(expert, h):
        names = slots(expert, begin[h], size[h])
        mix = jnp.where(names == target_one, route_ref[0:1, :], 0.0) + jnp.where(
            names == target_two, route_ref[1:2, :], 0.0
        )
        high = mix.astype(jnp.bfloat16)
        return high, (mix - high.astype(jnp.float32)).astype(jnp.bfloat16)

    def combine(expert, h):
        dims = (((0,), (0,)), ((), ()))
        high, low = weights_of(expert, h)
        values = home[expert, unit(h)]
        return lax.dot_general(
            high, values, dims, preferred_element_type=jnp.float32
        ) + lax.dot_general(low, values, dims, preferred_element_type=jnp.float32)

    def take_home(expert, h):
        with jax.named_scope("homewait"):
            home_arrival(expert, h).wait_recv()
        total[...] += combine(expert, h)

    def late_cross():
        for h in range(2):
            cross(at_step(1), h)

    def late_home():
        for h in range(2):
            send_home(at_step(1), h)

    pl.when(at_end)(late_cross)
    for h in range(2):
        cross(mine, h)
    for h in range(2):
        send_home(at_step(last), h)
    pl.when(at_end)(late_home)
    home[mine, unit(0)] = meet(mine, 0)
    total[...] = combine(mine, 0)
    for step in range(1, experts):
        take_home(at_step(step), 0)
    home[mine, unit(1)] = meet(mine, 1)
    total[...] += combine(mine, 1)
    for step in range(1, experts):
        take_home(at_step(step), 1)
    routed = total[...]
    sums[...] = jnp.broadcast_to(jnp.sum(routed * routed, axis=1, keepdims=True), (tok_rows, 128))
    sum_copy().start()
    with jax.named_scope("sum1"):
        sum_copy().wait_recv()
    squares_out = sums[...] + peer_sums[...]
    factor_out = lax.rsqrt(squares_out[:, 0:1] / (2 * width) + norm_eps)
    out_ref[...] = (total[...] * factor_out * gain_out_ref[:, own_cols]).astype(jnp.bfloat16)

    square_copy().wait_send()
    sum_copy().wait_send()

    def drain_own(side):
        own_note(side).wait_send()
        for p in range(2):
            own_copy(side, p).wait_send()

    for side in sides:
        pl.when(inside(mine + side))(functools.partial(drain_own, side))

    def drain_far(d):
        there = jnp.where(d < mine, mine + 1, mine - 1)

        def passed():
            note_copy(d, there).wait_send()
            for p in range(2):
                line_copy(d, p, there).wait_send()

        pl.when(inside(there))(passed)
        for h in range(2):
            home_copy(d, h).wait_send()

    def drain(d, carry):
        for i in range(2):
            core_copy(d, i, core).wait_send()
            pair_copy(d, i).wait_send()
            relay_copy(d, i, core).wait_send()
            part_copy(d, i).wait_send()
            cross_copy(d, i).wait_send()
        pl.when(d != mine)(lambda: drain_far(d))
        return carry

    lax.fori_loop(0, experts, drain, 0)


def layer(
    tokens, gain_in, gain_out, expert_ids, route_weight, gate_weight, up_weight, down_weight
):
    tok_rows, width = tokens.shape
    experts = lax.axis_size("ep") // 2
    picks = expert_ids.shape[1]
    cap = tok_rows * picks * 3 // (2 * experts)
    hidden_width = gate_weight.shape[2]
    if picks != 2 or experts < 3 or cap % 16 or cap < 32 or width % 256 or hidden_width % 128:
        return plain(
            tokens, gain_in, gain_out, expert_ids, route_weight, gate_weight, up_weight, down_weight
        )
    vmem = pl.BlockSpec(memory_space=pltpu.VMEM)
    hbm = pl.BlockSpec(memory_space=pl.ANY)
    bf16, f32 = jnp.bfloat16, jnp.float32
    lines = [pltpu.SemaphoreType.DMA((experts * 2,))] * 14
    return pl.pallas_call(
        functools.partial(fused, experts, cap),
        out_shape=jax.ShapeDtypeStruct((tok_rows, width), bf16),
        in_specs=[vmem] * 5 + [hbm] * 3,
        out_specs=vmem,
        scratch_shapes=[
            pltpu.VMEM((experts, tok_rows, width), bf16),
            pltpu.VMEM((experts, 8, tok_rows), f32),
            pltpu.VMEM((experts, 2, cap, 2 * width), bf16),
            pltpu.VMEM((experts, 2 * cap, 2 * width), bf16),
            pltpu.VMEM((experts, 2 * cap, width), bf16),
            pltpu.VMEM((experts, cap, width), bf16),
            pltpu.VMEM((experts, cap, width), bf16),
            pltpu.VMEM((experts, cap, width), bf16),
            pltpu.VMEM((experts, cap, width), bf16),
            pltpu.VMEM((2 * width, 2 * hidden_width), bf16),
            pltpu.VMEM((hidden_width, 2 * width), bf16),
            pltpu.VMEM((8, tok_rows), f32),
            pltpu.VMEM((8, tok_rows), f32),
            pltpu.VMEM((tok_rows, 128), f32),
            pltpu.VMEM((tok_rows, 128), f32),
            pltpu.VMEM((tok_rows, width), f32),
            pltpu.SemaphoreType.DMA((3,)),
            pltpu.SemaphoreType.DMA((2,)),
            pltpu.SemaphoreType.DMA((2,)),
            pltpu.SemaphoreType.DMA((4,)),
            pltpu.SemaphoreType.DMA((2,)),
            pltpu.SemaphoreType.DMA((experts,)),
            pltpu.SemaphoreType.DMA((experts,)),
        ]
        + lines,
        compiler_params=pltpu.CompilerParams(
            collective_id=0, has_side_effects=True, vmem_limit_bytes=60 * 1024 * 1024
        ),
    )(
        tokens,
        gain_in[None, :],
        gain_out[None, :],
        expert_ids.T,
        route_weight.T,
        gate_weight,
        up_weight,
        down_weight,
    )


def solution(mesh):
    in_specs = (
        P(("grp", "ep"), "tp"),
        P(),
        P(),
        P(("grp", "ep"), None),
        P(("grp", "ep"), None),
        P("ep", None, "tp"),
        P("ep", None, "tp"),
        P("ep", "tp", None),
    )
    out_specs = P(("grp", "ep"), "tp")
    return jax.shard_map(layer, mesh=mesh, in_specs=in_specs, out_specs=out_specs, check_vma=False)
```

profile of v0, /device:TPU:0, one launch (start us, length us, event | category | flops | bytes accessed | tf_op | source)
XLA Modules:
  0.0 73.2 jit_solution(1751647303315549556)
XLA Ops:
  0.0 71.4 %shard_map.82 = bf16[192,1024]{1,0:T(8,128)(2,1)} custom-call(bf16[192,1024]{1,0:T(8,128)(2,1)} %tok_ref.1, f32[1,2048]{1,0:T(1,128)} %bitcast.4, f32[1,2048]{1,0:T(1,128)} %bitcast.5, s32[2,192]{1,0:T(2,128)} %bitcast.6, f32[2,192]{1,0:T(2,128)} %bitcast.7, bf16[1,2048,896]{2,1,0:T(8,128)(2,1)} %gate_hbm.1, bf16[1,2048,896]{2,1,0:T(8,128)(2,1)} %up_hbm.1, ...), custom_call_target="tpu_custom_call" | custom-call | tf_op jit(solution)/shard_map/pallas_call | solution.py:559
  71.4 1.8 %copy.10 = bf16[192,1024]{1,0:T(8,128)(2,1)} copy(bf16[192,1024]{1,0:T(8,128)(2,1)} %shard_map.82) | data formatting | bytes 786432
where the time goes:
time: 73.4 us; the launch traced here: 73.2 us
  Pallas kernels  71.4 us (97%)
  local copies, waits for them, and re-layouts  1.77 us (2%)
    pallas_call x1, Pallas kernels, layer(): pl.pallas_call(functools.partial(fused, experts, cap), out_shape=jax.Shap...  71.4 us
    unnamed x1, local copies, waits for them, and re-layouts  1.77 us

commit v1 on v0

--- a/solution.py
+++ b/solution.py
@@ -76,17 +76,23 @@
 def fused(
     experts,
     cap,
+    tok_hbm,
+    gain_in_hbm,
+    gain_out_hbm,
+    ids_hbm,
+    route_hbm,
+    gate_hbm,
+    up_hbm,
+    down_hbm,
+    out_ref,
     tok_ref,
     gain_in_ref,
     gain_out_ref,
     ids_ref,
     route_ref,
-    gate_hbm,
-    up_hbm,
-    down_hbm,
-    out_ref,
     arrived,
     notes,
+    packed,
     rows,
     parts,
     peer_parts,
@@ -102,25 +108,18 @@
     peer_sums,
     total,
     w_sem,
-    sq_send,
+    in_sem,
+    sent,
+    own_sent,
+    line_sent,
+    note_sent,
     sq_recv,
-    own_send,
-    own_note_send,
-    note_send,
     note_recv,
-    line_send,
     line_recv,
-    core_send,
-    core_recv,
-    pair_send,
+    rows_recv,
     pair_recv,
-    relay_send,
-    relay_recv,
-    part_send,
     part_recv,
-    cross_send,
     cross_recv,
-    home_send,
     home_recv,
 ):
     tok_rows, width = tok_ref.shape
@@ -157,8 +156,15 @@
     def turn(where):
         return 1 - 2 * ((2 * where) // experts)
 
-    at_end = (mine == 0) | (mine == experts - 1)
-    inner = jnp.logical_not(at_end)
+    last = experts - 1
+
+    def is_end(where):
+        return (where == 0) | (where == last)
+
+    def is_inner(where):
+        return (where > 0) & (where < last)
+
+    at_end, inner = is_end(mine), is_inner(mine)
 
     def at_step(step):
         far = jnp.where(step == 2, experts - 1, jnp.where(step > 2, step - 1, step))
@@ -171,9 +177,9 @@
     loads = [
         pltpu.make_async_copy(gate_hbm.at[0], gate_up.at[:, pl.ds(0, hidden_width)], w_sem.at[0]),
         pltpu.make_async_copy(
-            up_hbm.at[0], gate_up.at[:, pl.ds(hidden_width, hidden_width)], w_sem.at[1]
+            up_hbm.at[0], gate_up.at[:, pl.ds(hidden_width, hidden_width)], w_sem.at[0]
         ),
-        pltpu.make_async_copy(down_hbm.at[0], down, w_sem.at[2]),
+        pltpu.make_async_copy(down_hbm.at[0], down, w_sem.at[1]),
     ]
     barrier = pltpu.get_barrier_semaphore()
     sides = (-1, 1)
@@ -189,7 +195,19 @@
         pl.when(inside(mine + side))(functools.partial(greet, side))
     pl.semaphore_signal(barrier, inc=1, device_id={"ep": partner}, device_id_type=MESH)
     pl.semaphore_signal(barrier, inc=1, device_id={"tp": other}, device_id_type=MESH)
-    for load in loads:
+    inputs = [
+        pltpu.make_async_copy(source, target, in_sem.at[i])
+        for i, (source, target) in enumerate(
+            (
+                (tok_hbm, tok_ref),
+                (ids_hbm, ids_ref),
+                (gain_in_hbm, gain_in_ref),
+                (route_hbm, route_ref),
+                (gain_out_hbm, gain_out_ref),
+            )
+        )
+    ]
+    for load in inputs:
         load.start()
 
     def remote(source, target, send, recv, device):
@@ -203,16 +221,16 @@
         )
 
     def square_copy():
-        return remote(squared, peer_squared, sq_send.at[0], sq_recv.at[0], {"tp": other})
+        return remote(squared, peer_squared, sent.at[0], sq_recv.at[0], {"tp": other})
 
     def sum_copy():
-        return remote(sums, peer_sums, sq_send.at[1], sq_recv.at[1], {"tp": other})
+        return remote(sums, peer_sums, sent.at[1], sq_recv.at[1], {"tp": other})
 
     def own_copy(side, p):
         return remote(
             tok_ref.at[:, cut(p)],
             arrived.at[mine, :, cut(p)],
-            own_send.at[side + 1 + p],
+            own_sent.at[(side + 1) // 2],
             line_recv.at[2 * mine + p],
             on_line(mine + side),
         )
@@ -221,41 +239,56 @@
         return remote(
             notes.at[mine],
             notes.at[mine],
-            own_note_send.at[(side + 1) // 2],
+            own_sent.at[2 + (side + 1) // 2],
             note_recv.at[mine],
             on_line(mine + side),
         )
 
     def line_copy(source, p, there):
-        view, sem = arrived.at[source, :, cut(p)], 2 * source + p
-        return remote(view, view, line_send.at[sem], line_recv.at[sem], on_line(there))
+        view = arrived.at[source, :, cut(p)]
+        return remote(
+            view, view, line_sent.at[source], line_recv.at[2 * source + p], on_line(there)
+        )
 
     def note_copy(source, there):
         view = notes.at[source]
-        return remote(view, view, note_send.at[source], note_recv.at[source], on_line(there))
-
-    def core_copy(d, p, which):
-        view, sem = rows.at[d, 0, :, of_core(which, p)], 2 * d + p
-        return remote(view, view, core_send.at[sem], core_recv.at[sem], {"tp": other})
+        return remote(view, view, note_sent.at[source], note_recv.at[source], on_line(there))
+
+    def box_copy(source, p, there):
+        return remote(
+            packed.at[source, :, cut(p)],
+            rows.at[source, 0, :, of_core(core, p)],
+            sent.at[3],
+            line_recv.at[2 * source + p],
+            on_line(there),
+        )
+
+    def core_copy(d, p):
+        view = rows.at[d, 0, :, of_core(core, p)]
+        return remote(view, view, sent.at[4], rows_recv.at[d], {"tp": other})
 
     def pair_copy(d, p):
         return remote(
             rows.at[d, 0, :, of_core(core, p)],
             rows.at[d, 1, :, of_core(core, p)],
-            pair_send.at[2 * d + p],
+            sent.at[5],
             pair_recv.at[2 * d + p],
             {"ep": partner},
         )
 
-    def relay_copy(d, p, which):
-        view, sem = rows.at[d, 1, :, of_core(which, p)], 2 * d + p
-        return remote(view, view, relay_send.at[sem], relay_recv.at[sem], {"tp": other})
+    def relay_copy(d, p):
+        view = rows.at[d, 1, :, of_core(core, p)]
+        return remote(view, view, sent.at[4], rows_recv.at[d], {"tp": other})
+
+    def other_half(d):
+        view = rows.at[d, :, :, other_cols]
+        return remote(view, view, sent.at[4], rows_recv.at[d], {"tp": other})
 
     def part_copy(d, h):
         return remote(
             parts.at[d, both(h), other_cols],
             peer_parts.at[d, both(h)],
-            part_send.at[2 * d + h],
+            sent.at[6],
             part_recv.at[2 * d + h],
             {"tp": other},
         )
@@ -264,7 +297,7 @@
         return remote(
             crossing.at[d, unit(h)],
             crossed.at[d, unit(h)],
-            cross_send.at[2 * d + h],
+            sent.at[7],
             cross_recv.at[2 * d + h],
             {"ep": partner},
         )
@@ -273,20 +306,39 @@
         return remote(
             leaving.at[d, unit(h)],
             home.at[mine, unit(h)],
-            home_send.at[2 * d + h],
+            sent.at[8],
             home_recv.at[2 * mine + h],
             on_line(d),
         )
 
     def home_arrival(expert, h):
-        view, sem = home.at[expert, unit(h)], 2 * expert + h
-        return remote(view, view, home_send.at[sem], home_recv.at[sem], on_line(expert))
-
+        view = home.at[expert, unit(h)]
+        return remote(view, view, sent.at[8], home_recv.at[2 * expert + h], on_line(expert))
+
+    inputs[0].wait()
+    with jax.named_scope("barrier"):
+        pl.semaphore_wait(
+            barrier, 2 + (mine > 0).astype(jnp.int32) + (mine < experts - 1).astype(jnp.int32)
+        )
+
+    def own_out(side, p):
+        own_copy(side, p).start()
+
+    def own_note_out(side):
+        own_note(side).start()
+
+    for side in sides:
+        pl.when(is_inner(mine + side))(functools.partial(own_out, side, 0))
     own_float = tok_ref[...].astype(jnp.float32)
     squares = jnp.broadcast_to(
         jnp.sum(own_float * own_float, axis=1, keepdims=True), (tok_rows, 128)
     )
     squared[...] = squares.T[0:8, :]
+    square_copy().start()
+    for load in loads:
+        load.start()
+    for load in inputs[1:]:
+        load.wait()
     lead = max(8, experts)
     names = lax.broadcasted_iota(jnp.int32, (lead, tok_rows), 0)
     first = names == ids_ref[0:1, :]
@@ -306,58 +358,67 @@
         names = lax.broadcasted_iota(jnp.int32, (count, tok_rows), 0) + expert * cap + first_row
         return names.astype(jnp.float32)
 
-    with jax.named_scope("barrier"):
-        pl.semaphore_wait(
-            barrier, 2 + (mine > 0).astype(jnp.int32) + (mine < experts - 1).astype(jnp.int32)
-        )
-    square_copy().start()
-
-    def own_out(side, p):
-        own_copy(side, p).start()
-
-    def own_note_out(side):
-        own_note(side).start()
-
-    for side in sides:
-        pl.when(inside(mine + side))(functools.partial(own_out, side, 0))
     with jax.named_scope("sum0"):
         square_copy().wait_recv()
     factor = lax.rsqrt((squared[...] + peer_squared[...]) / (2 * width) + norm_eps)
     row = lax.broadcasted_iota(jnp.int32, (8, tok_rows), 0)
     notes[mine] = jnp.where(row == 0, target_one, jnp.where(row == 1, target_two, factor))
     for side in sides:
-        pl.when(inside(mine + side))(functools.partial(own_note_out, side))
+        pl.when(is_inner(mine + side))(functools.partial(own_note_out, side))
     for side in sides:
-        pl.when(inside(mine + side))(functools.partial(own_out, side, 1))
-
-    def fill(source, p, tokens):
+        pl.when(is_inner(mine + side))(functools.partial(own_out, side, 1))
+
+    def pack(source, p, tokens, expert):
         one, two, scale = (notes[source, i : i + 1, :] for i in range(3))
-        names = slots(mine, 0, cap)
+        names = slots(expert, 0, cap)
         placing = jnp.where((names == one) | (names == two), scale, 0.0)
         high = placing.astype(jnp.bfloat16)
         low = (placing - high.astype(jnp.float32)).astype(jnp.bfloat16)
         values = jnp.dot(high, tokens, preferred_element_type=jnp.float32) + jnp.dot(
             low, tokens, preferred_element_type=jnp.float32
         )
-        rows[source, 0, :, of_core(core, p)] = (
-            values * gain_in_ref[:, of_core(core, p)]
-        ).astype(jnp.bfloat16)
+        return (values * gain_in_ref[:, of_core(core, p)]).astype(jnp.bfloat16)
+
+    def launch(source, p):
         pair_copy(source, p).start()
-        core_copy(source, p, core).start()
+        core_copy(source, p).start()
 
     def fill_step(step, p):
         source = at_step(step)
-        fill(source, p, arrived[source, :, cut(p)])
+
+        def fill():
+            rows[source, 0, :, of_core(core, p)] = pack(
+                source, p, arrived[source, :, cut(p)], mine
+            )
+
+        pl.when(inner)(fill)
+        launch(source, p)
+
+    def box_out(source, p, tokens, there):
+        packed[source, :, cut(p)] = pack(source, p, tokens, there)
+        box_copy(source, p, there).start()
 
     def pass_on(step, side, p):
         source, there = mine + side * step, mine - side
-        with jax.named_scope("linewait"):
-            line_copy(source, p, mine).wait_recv()
-        pl.when(inside(there))(lambda: line_copy(source, p, there).start())
-        if p == 0:
-            with jax.named_scope("notewait"):
-                note_copy(source, mine).wait_recv()
-            pl.when(inside(there))(lambda: note_copy(source, there).start())
+
+        def take_box():
+            with jax.named_scope("boxwait"):
+                box_copy(source, p, mine).wait_recv()
+
+        def take_tokens():
+            with jax.named_scope("linewait"):
+                line_copy(source, p, mine).wait_recv()
+            pl.when(is_inner(there))(lambda: line_copy(source, p, there).start())
+            if p == 0:
+                with jax.named_scope("notewait"):
+                    note_copy(source, mine).wait_recv()
+                pl.when(is_inner(there))(lambda: note_copy(source, there).start())
+            pl.when(is_end(there))(
+                lambda: box_out(source, p, arrived[source, :, cut(p)], there)
+            )
+
+        pl.when(at_end)(take_box)
+        pl.when(inner)(take_tokens)
 
     def take_line(step, p):
         for side in sides:
@@ -367,13 +428,11 @@
         for p in range(2):
             with jax.named_scope("pairwait"):
                 pair_copy(d, p).wait_recv()
-            relay_copy(d, p, core).start()
+            relay_copy(d, p).start()
 
     def take_core(d):
         with jax.named_scope("corewait"):
-            for p in range(2):
-                core_copy(d, p, other).wait_recv()
-                relay_copy(d, p, other).wait_recv()
+            other_half(d).wait_recv()
 
     def compute(d, h):
         block = jnp.concatenate([rows[d, 0, unit(h), :], rows[d, 1, unit(h), :]], axis=0)
@@ -410,7 +469,13 @@
 
     last = experts - 1
     for p in range(2):
-        fill(mine, p, tok_ref[:, cut(p)])
+        rows[mine, 0, :, of_core(core, p)] = pack(mine, p, tok_ref[:, cut(p)], mine)
+        launch(mine, p)
+        for side in sides:
+            there = mine + side
+            pl.when(inner & is_end(there))(
+                functools.partial(lambda p, there: box_out(mine, p, tok_ref[:, cut(p)], there), p, there)
+            )
     take_line(1, 0)
     fill_step(1, 0)
     take_pair(mine)
@@ -423,31 +488,33 @@
 
     pl.when(inner)(lambda: fill_both(2))
     with jax.named_scope("wwait"):
-        for load in loads:
-            load.wait()
+        pltpu.make_async_copy(gate_up, gate_up, w_sem.at[0]).wait()
+        loads[2].wait()
 
     def step_of(d, carry):
         now, past = at_step(d), at_step(d - 1)
         early = (d >= 2) | ((d == 1) & inner)
-        early_past = (d >= 3) | ((d == 2) & inner)
 
         def next_line():
             take_line(d + 1, 1)
             pl.when(at_end)(lambda: fill_step(d + 1, 1))
+            pl.when(inner & (d + 2 <= last))(lambda: fill_step(d + 2, 1))
 
         pl.when(d >= 1)(lambda: take_pair(now))
-        pl.when((d >= 2) & (d < last))(next_line)
+        pl.when((d >= 1) & (d < last) & (at_end | (d >= 2)))(next_line)
         take_core(now)
         compute(now, 0)
-        pl.when(early_past)(lambda: send_home(past, 0))
-        pl.when(d == 1)(next_line)
+        pl.when((d >= 3) & inner)(lambda: send_home(at_step(d - 2), 1))
+        pl.when((d >= 3) & at_end)(lambda: send_home(past, 0))
+        pl.when((d == 1) & inner)(next_line)
         compute(now, 1)
         pl.when(early)(lambda: cross(now, 0))
+        pl.when((d >= 2) & inner)(lambda: send_home(past, 0))
+        pl.when((d >= 3) & at_end)(lambda: send_home(past, 1))
         pl.when(d + 2 <= last)(lambda: take_line(d + 2, 0))
-        pl.when(early_past)(lambda: send_home(past, 1))
         pl.when(early)(lambda: cross(now, 1))
         pl.when((d + 2 <= last) & at_end)(lambda: fill_step(d + 2, 0))
-        pl.when((d >= 1) & (d + 2 <= last) & inner)(lambda: fill_both(d + 2))
+        pl.when((d + 3 <= last) & inner)(lambda: fill_step(d + 3, 0))
         return carry
 
     lax.fori_loop(0, experts, step_of, 0)
@@ -473,27 +540,32 @@
             home_arrival(expert, h).wait_recv()
         total[...] += combine(expert, h)
 
-    def late_cross():
+    def end_rest():
         for h in range(2):
             cross(at_step(1), h)
-
-    def late_home():
         for h in range(2):
-            send_home(at_step(1), h)
-
-    pl.when(at_end)(late_cross)
-    for h in range(2):
-        cross(mine, h)
-    for h in range(2):
-        send_home(at_step(last), h)
-    pl.when(at_end)(late_home)
+            cross(mine, h)
+        for step in (last, 1):
+            for h in range(2):
+                send_home(at_step(step), h)
+
+    def inner_rest():
+        for h in range(2):
+            cross(mine, h)
+        send_home(at_step(last - 1), 1)
+        for h in range(2):
+            send_home(at_step(last), h)
+
+    pl.when(at_end)(end_rest)
+    pl.when(inner)(inner_rest)
     home[mine, unit(0)] = meet(mine, 0)
     total[...] = combine(mine, 0)
-    for step in range(1, experts):
+    waited = [step for step in range(1, experts) if step != 2] + [2] * (experts > 2)
+    for step in waited:
         take_home(at_step(step), 0)
     home[mine, unit(1)] = meet(mine, 1)
     total[...] += combine(mine, 1)
-    for step in range(1, experts):
+    for step in waited:
         take_home(at_step(step), 1)
     routed = total[...]
     sums[...] = jnp.broadcast_to(jnp.sum(routed * routed, axis=1, keepdims=True), (tok_rows, 128))
@@ -504,40 +576,43 @@
     factor_out = lax.rsqrt(squares_out[:, 0:1] / (2 * width) + norm_eps)
     out_ref[...] = (total[...] * factor_out * gain_out_ref[:, own_cols]).astype(jnp.bfloat16)
 
+    def sent_all(view, sem):
+        pltpu.make_async_remote_copy(
+            src_ref=view,
+            dst_ref=view,
+            send_sem=sem,
+            recv_sem=sq_recv.at[0],
+            device_id={"tp": other},
+            device_id_type=MESH,
+        ).wait_send()
+
+    others = pl.ds(0, last)
+    for side in sides:
+
+        def own_done(side=side):
+            sent_all(tok_ref, own_sent.at[(side + 1) // 2])
+            own_note(side).wait_send()
+
+        pl.when(is_inner(mine + side))(own_done)
+        pl.when(inner & is_end(mine + side))(lambda: sent_all(packed.at[others], sent.at[3]))
+
+    def forwarded(source, carry):
+        def done():
+            sent_all(notes.at[source], note_sent.at[source])
+            sent_all(arrived.at[source], line_sent.at[source])
+
+        up = (source < mine) & is_inner(mine + 1)
+        pl.when(inner & (up | ((source > mine) & is_inner(mine - 1))))(done)
+        return carry
+
+    lax.fori_loop(0, experts, forwarded, 0)
+    sent_all(rows.at[:, :, :, pl.ds(0, width)], sent.at[4])
+    sent_all(rows.at[:, 0, :, pl.ds(0, width)], sent.at[5])
+    sent_all(parts.at[:, :, pl.ds(0, width)], sent.at[6])
+    sent_all(crossing, sent.at[7])
+    sent_all(leaving.at[others], sent.at[8])
     square_copy().wait_send()
     sum_copy().wait_send()
-
-    def drain_own(side):
-        own_note(side).wait_send()
-        for p in range(2):
-            own_copy(side, p).wait_send()
-
-    for side in sides:
-        pl.when(inside(mine + side))(functools.partial(drain_own, side))
-
-    def drain_far(d):
-        there = jnp.where(d < mine, mine + 1, mine - 1)
-
-        def passed():
-            note_copy(d, there).wait_send()
-            for p in range(2):
-                line_copy(d, p, there).wait_send()
-
-        pl.when(inside(there))(passed)
-        for h in range(2):
-            home_copy(d, h).wait_send()
-
-    def drain(d, carry):
-        for i in range(2):
-            core_copy(d, i, core).wait_send()
-            pair_copy(d, i).wait_send()
-            relay_copy(d, i, core).wait_send()
-            part_copy(d, i).wait_send()
-            cross_copy(d, i).wait_send()
-        pl.when(d != mine)(lambda: drain_far(d))
-        return carry
-
-    lax.fori_loop(0, experts, drain, 0)
 
 
 def layer(
@@ -548,22 +623,28 @@
     picks = expert_ids.shape[1]
     cap = tok_rows * picks * 3 // (2 * experts)
     hidden_width = gate_weight.shape[2]
-    if picks != 2 or experts < 3 or cap % 16 or cap < 32 or width % 256 or hidden_width % 128:
+    if picks != 2 or experts < 4 or cap % 16 or cap < 32 or width % 256 or hidden_width % 128:
         return plain(
             tokens, gain_in, gain_out, expert_ids, route_weight, gate_weight, up_weight, down_weight
         )
     vmem = pl.BlockSpec(memory_space=pltpu.VMEM)
     hbm = pl.BlockSpec(memory_space=pl.ANY)
     bf16, f32 = jnp.bfloat16, jnp.float32
-    lines = [pltpu.SemaphoreType.DMA((experts * 2,))] * 14
+    dma = pltpu.SemaphoreType.DMA
     return pl.pallas_call(
         functools.partial(fused, experts, cap),
-        out_shape=jax.ShapeDtypeStruct((tok_rows, width), bf16),
-        in_specs=[vmem] * 5 + [hbm] * 3,
+        out_shape=pltpu.VMEM((tok_rows, width), bf16),
+        in_specs=[hbm] * 8,
         out_specs=vmem,
         scratch_shapes=[
+            pltpu.VMEM((tok_rows, width), bf16),
+            pltpu.VMEM((1, 2 * width), f32),
+            pltpu.VMEM((1, 2 * width), f32),
+            pltpu.VMEM((picks, tok_rows), jnp.int32),
+            pltpu.VMEM((picks, tok_rows), f32),
             pltpu.VMEM((experts, tok_rows, width), bf16),
             pltpu.VMEM((experts, 8, tok_rows), f32),
+            pltpu.VMEM((experts, cap, width), bf16),
             pltpu.VMEM((experts, 2, cap, 2 * width), bf16),
             pltpu.VMEM((experts, 2 * cap, 2 * width), bf16),
             pltpu.VMEM((experts, 2 * cap, width), bf16),
@@ -578,15 +659,21 @@
             pltpu.VMEM((tok_rows, 128), f32),
             pltpu.VMEM((tok_rows, 128), f32),
             pltpu.VMEM((tok_rows, width), f32),
-            pltpu.SemaphoreType.DMA((3,)),
-            pltpu.SemaphoreType.DMA((2,)),
-            pltpu.SemaphoreType.DMA((2,)),
-            pltpu.SemaphoreType.DMA((4,)),
-            pltpu.SemaphoreType.DMA((2,)),
-            pltpu.SemaphoreType.DMA((experts,)),
-            pltpu.SemaphoreType.DMA((experts,)),
-        ]
-        + lines,
+            dma((2,)),
+            dma((5,)),
+            dma((9,)),
+            dma((4,)),
+            dma((experts,)),
+            dma((experts,)),
+            dma((2,)),
+            dma((experts,)),
+            dma((2 * experts,)),
+            dma((experts,)),
+            dma((2 * experts,)),
+            dma((2 * experts,)),
+            dma((2 * experts,)),
+            dma((2 * experts,)),
+        ],
         compiler_params=pltpu.CompilerParams(
             collective_id=0, has_side_effects=True, vmem_limit_bytes=60 * 1024 * 1024
         ),

time: 73.4 us -> 67.6 us (0.921)
  Pallas kernels: 71.4 us -> 66.7 us
  local copies, waits for them, and re-layouts: 1.77 us -> 0.75 us
    pallas_call x1, Pallas kernels: 71.4 us -> 66.7 us  [layer(): pl.pallas_call(functools.partial(fused, experts, cap), out_shape=pltpu.VM...]
    unnamed x1, local copies, waits for them, and re-layouts: 1.77 us -> 0.75 us
where the time goes in v1:
time: 67.6 us; the launch traced here: 67.4 us
  Pallas kernels  66.7 us (99%)
  local copies, waits for them, and re-layouts  0.75 us (1%)
    pallas_call x1, Pallas kernels, layer(): pl.pallas_call(functools.partial(fused, experts, cap), out_shape=pltpu.VM...  66.7 us

profile of v1, /device:TPU:0, one launch (start us, length us, event | category | flops | bytes accessed | tf_op | source)
XLA Modules:
  0.0 67.4 jit_solution(9261393325329611594)
XLA Ops:
  0.0 66.7 %shard_map.82 = bf16[192,1024]{1,0:T(8,128)(2,1)S(1)} custom-call(bf16[192,1024]{1,0:T(8,128)(2,1)} %tok_hbm.1, f32[1,2048]{1,0:T(1,128)} %bitcast.4, f32[1,2048]{1,0:T(1,128)} %bitcast.5, s32[2,192]{1,0:T(2,128)} %bitcast.6, f32[2,192]{1,0:T(2,128)} %bitcast.7, bf16[1,2048,896]{2,1,0:T(8,128)(2,1)} %gate_hbm.1, bf16[1,2048,896]{2,1,0:T(8,128)(2,1)} %up_hbm.1, ...), custom_call_target="tpu_custom_call" | custom-call | tf_op jit(solution)/shard_map/pallas_call | solution.py:634
  66.7 0.7 %copy.10 = bf16[192,1024]{1,0:T(8,128)(2,1)} copy(bf16[192,1024]{1,0:T(8,128)(2,1)S(1)} %shard_map.82) | data formatting | bytes 786432

commit v2 on v1

--- a/solution.py
+++ b/solution.py
@@ -500,15 +500,21 @@
             pl.when(at_end)(lambda: fill_step(d + 1, 1))
             pl.when(inner & (d + 2 <= last))(lambda: fill_step(d + 2, 1))
 
+        def line_after():
+            take_line(d + 2, 0)
+            pl.when(at_end)(lambda: fill_step(d + 2, 0))
+            pl.when(inner & (d + 3 <= last))(lambda: fill_step(d + 3, 0))
+
         pl.when(d >= 1)(lambda: take_pair(now))
         pl.when((d >= 1) & (d < last) & (at_end | (d >= 2)))(next_line)
         take_core(now)
         compute(now, 0)
         pl.when((d >= 3) & inner)(lambda: send_home(at_step(d - 2), 1))
         pl.when((d >= 3) & at_end)(lambda: send_home(past, 0))
+        pl.when((d == last) & at_end)(lambda: cross(now, 0))
         pl.when((d == 1) & inner)(next_line)
         compute(now, 1)
-        pl.when(early)(lambda: cross(now, 0))
+        pl.when(early & ((d < last) | inner))(lambda: cross(now, 0))
         pl.when((d >= 2) & inner)(lambda: send_home(past, 0))
         pl.when((d >= 3) & at_end)(lambda: send_home(past, 1))
         pl.when(d + 2 <= last)(lambda: take_line(d + 2, 0))
@@ -527,18 +533,19 @@
         high = mix.astype(jnp.bfloat16)
         return high, (mix - high.astype(jnp.float32)).astype(jnp.bfloat16)
 
-    def combine(expert, h):
+    def combine(expert, h, mixes=None):
         dims = (((0,), (0,)), ((), ()))
-        high, low = weights_of(expert, h)
+        high, low = mixes or weights_of(expert, h)
         values = home[expert, unit(h)]
         return lax.dot_general(
             high, values, dims, preferred_element_type=jnp.float32
         ) + lax.dot_general(low, values, dims, preferred_element_type=jnp.float32)
 
     def take_home(expert, h):
+        mixes = weights_of(expert, h)
         with jax.named_scope("homewait"):
             home_arrival(expert, h).wait_recv()
-        total[...] += combine(expert, h)
+        total[...] += combine(expert, h, mixes)
 
     def end_rest():
         for h in range(2):
@@ -568,12 +575,14 @@
     for step in waited:
         take_home(at_step(step), 1)
     routed = total[...]
-    sums[...] = jnp.broadcast_to(jnp.sum(routed * routed, axis=1, keepdims=True), (tok_rows, 128))
+    sums[...] = jnp.broadcast_to(
+        jnp.sum(routed * routed, axis=1, keepdims=True), (tok_rows, 128)
+    ).T[0:8, :]
     sum_copy().start()
     with jax.named_scope("sum1"):
         sum_copy().wait_recv()
     squares_out = sums[...] + peer_sums[...]
-    factor_out = lax.rsqrt(squares_out[:, 0:1] / (2 * width) + norm_eps)
+    factor_out = lax.rsqrt(squares_out / (2 * width) + norm_eps).T[:, 0:1]
     out_ref[...] = (total[...] * factor_out * gain_out_ref[:, own_cols]).astype(jnp.bfloat16)
 
     def sent_all(view, sem):
@@ -656,8 +665,8 @@
             pltpu.VMEM((hidden_width, 2 * width), bf16),
             pltpu.VMEM((8, tok_rows), f32),
             pltpu.VMEM((8, tok_rows), f32),
-            pltpu.VMEM((tok_rows, 128), f32),
-            pltpu.VMEM((tok_rows, 128), f32),
+            pltpu.VMEM((8, tok_rows), f32),
+            pltpu.VMEM((8, tok_rows), f32),
             pltpu.VMEM((tok_rows, width), f32),
             dma((2,)),
             dma((5,)),

time: 67.6 us -> 67.5 us (level)
  no operation moved by 1% of the time
where the time goes in v2:
time: 67.5 us; the launch traced here: 67.4 us
  Pallas kernels  66.6 us (99%)
  local copies, waits for them, and re-layouts  0.75 us (1%)
    pallas_call x1, Pallas kernels, layer(): pl.pallas_call(functools.partial(fused, experts, cap), out_shape=pltpu.VM...  66.6 us

profile of v2, /device:TPU:0, one launch (start us, length us, event | category | flops | bytes accessed | tf_op | source)
XLA Modules:
  0.0 67.4 jit_solution(10262620711030937200)
XLA Ops:
  0.0 66.6 %shard_map.82 = bf16[192,1024]{1,0:T(8,128)(2,1)S(1)} custom-call(bf16[192,1024]{1,0:T(8,128)(2,1)} %tok_hbm.1, f32[1,2048]{1,0:T(1,128)} %bitcast.4, f32[1,2048]{1,0:T(1,128)} %bitcast.5, s32[2,192]{1,0:T(2,128)} %bitcast.6, f32[2,192]{1,0:T(2,128)} %bitcast.7, bf16[1,2048,896]{2,1,0:T(8,128)(2,1)} %gate_hbm.1, bf16[1,2048,896]{2,1,0:T(8,128)(2,1)} %up_hbm.1, ...), custom_call_target="tpu_custom_call" | custom-call | tf_op jit(solution)/shard_map/pallas_call | solution.py:643
  66.6 0.7 %copy.10 = bf16[192,1024]{1,0:T(8,128)(2,1)} copy(bf16[192,1024]{1,0:T(8,128)(2,1)S(1)} %shard_map.82) | data formatting | bytes 786432
